TPU v7x, 32 devices: a whole 2x2x4 slice. The times are simulated.
32 devices in a mesh: sp: 16 (over z, y, x), tp: 2 (over core).
Axes of the slice: x: 2, y: 2, z: 4, core: 2. Of those that a mesh axis runs over, the one named last changes fastest.
Arguments:
- resid: bfloat16 [6144, 2048], P('sp', 'tp'), may hold values from -40 to 40
- query_one: bfloat16 [6144, 1024], P('sp', 'tp'), may hold values from -64 to 64
- key_one: bfloat16 [6144, 1024], P('sp', 'tp'), may hold values from -64 to 64
- query_two: bfloat16 [6144, 1024], P('sp', 'tp'), may hold values from -64 to 64
- key_two: bfloat16 [6144, 1024], P('sp', 'tp'), may hold values from -64 to 64
- values: bfloat16 [6144, 2048], P('sp', 'tp'), may hold values from -6 to 6
- mix_lambda: float32 [8], P('tp'), may hold values from 0.3 to 0.8
- segments: int32 [6144], P('sp'), may hold values from 0 to 7, never falling along the last dimension, each value on 1 to 1536 neighbouring positions
- head_gain: float32 [256], replicated, may hold values from 0.1 to 1.9
- out_weight: bfloat16 [2048, 2048], P(None, 'tp'), may hold values from -0.125 to 0.125
- mixer_gain: float32 [2048], P('tp'), may hold values from 0.1 to 1.9
- gate_weight: bfloat16 [2048, 6144], P('sp', 'tp'), may hold values from -0.125 to 0.125
- up_weight: bfloat16 [2048, 6144], P('sp', 'tp'), may hold values from -0.125 to 0.125
- down_weight: bfloat16 [6144, 2048], P('tp', 'sp'), may hold values from -0.078125 to 0.078125
Outputs:
- layer_out: bfloat16 [6144, 2048], P('sp', 'tp')
Inputs may be any that keep to these rules, and one draw needn't show every extreme that they name: `segments`: numbers never fall along the sequence; each document has at most 1536 positions and one has exactly that many.
All inputs are finite; a program needn't handle non-finite values.
Results may differ from a plain program's by a relative error of at most 0.012.
Values may be sent and summed in bfloat16 or wider, within the bound.
A program may use at most 128 MiB of HBM per device.

v0:
```python
import jax
import jax.numpy as jnp
from jax import lax
from jax.sharding import PartitionSpec as P

HD = 128
VD = 256
REACH = 4


def shifted(value, axis, by):
    length = lax.axis_size(axis)
    pairs = [(i, i + by) for i in range(length) if 0 <= i + by < length]
    return lax.ppermute(value, axis, pairs)


def body(
    resid,
    query_one,
    key_one,
    query_two,
    key_two,
    values,
    mix_lambda,
    segments,
    head_gain,
    out_weight,
    mixer_gain,
    gate_weight,
    up_weight,
    down_weight,
):
    rows = query_one.shape[0]
    heads = mix_lambda.shape[0]
    position = lax.axis_index("sp")
    carried = (key_one, key_two, values, segments)
    earlier = [carried]
    for step in range(REACH):
        carried = shifted((carried[0], carried[1], carried[2], carried[3]), "sp", 1)
        earlier.insert(0, carried)
    width = (REACH + 1) * rows
    k_first = jnp.concatenate([piece[0] for piece in earlier], 0).reshape(width, heads, HD)
    k_second = jnp.concatenate([piece[1] for piece in earlier], 0).reshape(width, heads, HD)
    vals = jnp.concatenate([piece[2] for piece in earlier], 0).reshape(width, heads, VD)
    seg_key = jnp.concatenate([piece[3] for piece in earlier], 0)
    q_pos = position * rows + jnp.arange(rows, dtype=jnp.int32)
    k_pos = (position - REACH) * rows + jnp.arange(width, dtype=jnp.int32)
    allowed = (
        (seg_key[None, :] == segments[:, None])
        & (k_pos[None, :] <= q_pos[:, None])
        & (k_pos[None, :] >= 0)
    )

    def weights(query, keys):
        score = jnp.einsum(
            "qhd,khd->hqk", query.reshape(rows, heads, HD), keys, preferred_element_type=jnp.float32
        ) * HD ** (-0.5)
        score = jnp.where(allowed[None], score, -jnp.inf)
        score = score - jnp.max(score, axis=-1, keepdims=True)
        expo = jnp.exp(score)
        return (expo / jnp.sum(expo, axis=-1, keepdims=True)).astype(jnp.bfloat16)

    out_first = jnp.einsum(
        "hqk,khe->qhe", weights(query_one, k_first), vals, preferred_element_type=jnp.float32
    )
    out_second = jnp.einsum(
        "hqk,khe->qhe", weights(query_two, k_second), vals, preferred_element_type=jnp.float32
    )
    head_out = out_first - mix_lambda[None, :, None] * out_second
    meansq = jnp.mean(head_out * head_out, axis=-1, keepdims=True)
    attn_rows = (
        (head_out * lax.rsqrt(meansq + 1e-05) * head_gain)
        .reshape(rows, heads * VD)
        .astype(jnp.bfloat16)
    )
    projected = jnp.dot(
        lax.all_gather(attn_rows, "tp", axis=1, tiled=True),
        out_weight,
        preferred_element_type=jnp.float32,
    )
    mid = (resid.astype(jnp.float32) + projected).astype(jnp.bfloat16)
    midf = mid.astype(jnp.float32)
    squares = lax.psum(jnp.sum(midf * midf, axis=1), "tp")
    channels = mid.shape[1] * lax.axis_size("tp")
    normed = (midf * lax.rsqrt(squares / channels + 1e-06)[:, None] * mixer_gain).astype(
        jnp.bfloat16
    )
    whole_rows = lax.all_gather(normed, "tp", axis=1, tiled=True)
    gate = jnp.dot(
        whole_rows,
        lax.all_gather(gate_weight, "sp", axis=0, tiled=True),
        preferred_element_type=jnp.float32,
    )
    up = jnp.dot(
        whole_rows,
        lax.all_gather(up_weight, "sp", axis=0, tiled=True),
        preferred_element_type=jnp.float32,
    )
    hidden = (jax.nn.silu(gate) * up).astype(jnp.bfloat16)
    terms = jnp.dot(
        hidden,
        lax.all_gather(down_weight, "sp", axis=1, tiled=True),
        preferred_element_type=jnp.float32,
    )
    summed = lax.psum_scatter(
        terms.astype(jnp.bfloat16), "tp", scatter_dimension=1, tiled=True
    ).astype(jnp.float32)
    return (midf + summed).astype(jnp.bfloat16)


def solution(mesh):
    in_specs = (
        P("sp", "tp"),
        P("sp", "tp"),
        P("sp", "tp"),
        P("sp", "tp"),
        P("sp", "tp"),
        P("sp", "tp"),
        P("tp"),
        P("sp"),
        P(),
        P(None, "tp"),
        P("tp"),
        P("sp", "tp"),
        P("sp", "tp"),
        P("tp", "sp"),
    )
    out_specs = P("sp", "tp")
    return jax.shard_map(body, mesh=mesh, in_specs=in_specs, out_specs=out_specs, check_vma=False)
```

profile of v0, /device:TPU:0, one launch (start us, length us, event | category | flops | bytes accessed | tf_op | source)
XLA Modules:
  0.0 768.8 jit_solution(17959958012359783923)
XLA Ops:
  7.8 4.9 collective-permute-start.12
  31.0 16.5 %collective-permute-done.5 = s32[384]{0:T(512)S(1)} collective-permute-done((s32[384]{0:T(512)S(1)}, s32[384]{0:T(512)S(1)}, u32[]{:S(2)}, u32[]{:S(2)}) %collective-permute-start.5) | collective-permute-done | bytes 1568 | tf_op jit(solution)/shard_map/ppermute | solution.py:14
  64.9 5.1 collective-permute-start.14
  74.4 5.9 collective-permute-start.10
  82.8 5.1 collective-permute-start.15
  90.5 5.3 collective-permute-start.1
  102.2 6.2 fusion.19
  108.4 17.4 %fusion.30 = (f32[4,384]{1,0:T(4,128)S(1)}, f32[4,384,1920]{1,2,0:T(8,128)}) fusion(f32[4,1920,384]{2,1,0:T(8,128)} %fusion.19, pred[384,1920]{0,1:T(8,128)(4,1)S(1)} %and_and_fusion), kind=kOutput, calls=%fused_computation.71 | output fusion | flops 17696640 | bytes 24336384 | tf_op jit(solution)/shard_map/sub | solution.py:59
  125.7 5.6 collective-permute-start.2
  134.7 6.1 fusion.22
  143.1 5.5 collective-permute-start.3
  148.6 17.7 %fusion.31 = (f32[4,384]{1,0:T(4,128)S(1)}, f32[4,384,1920]{1,2,0:T(8,128)}) fusion(f32[4,1920,384]{2,1,0:T(8,128)} %fusion.22, pred[384,1920]{0,1:T(8,128)(4,1)} %copy-done.4), kind=kOutput, calls=%fused_computation.72 | output fusion | flops 17696640 | bytes 24336384 | tf_op jit(solution)/shard_map/sub | solution.py:59
  171.1 6.3 copy.20
  177.4 8.0 %fusion.9 = f32[4,256,384]{2,1,0:T(8,128)S(1)} fusion(bf16[1920,4,256]{0,2,1:T(8,128)(2,1)} %bitcast.60, f32[4,384,1920]{1,2,0:T(8,128)} %get-tuple-element.6, f32[4,384]{1,0:T(4,128)S(1)} %get-tuple-element.5), kind=kOutput, calls=%fused_computation.15 | convolution fusion | flops 1515847680 | bytes 17307648 | tf_op jit(solution)/shard_map/hqk,khe->qhe/dot_general | solution.py:66
  185.4 6.8 fusion.16
  193.6 14.5 %all-gather.6.cloned.1.call-done = bf16[384,2048]{0,1:T(8,128)(2,1)} async-done(((bf16[384,1024]{0,1:T(8,128)(2,1)}), bf16[384,2048]{0,1:T(8,128)(2,1)}) %all-gather.6.cloned.1.call-update) | async-done | bytes 1572880 | tf_op jit(solution)/shard_map/all_gather | solution.py:77
  208.1 4.6 fusion.12
  218.3 9.2 %all-gather.8.cloned.1.call-done = bf16[384,2048]{1,0:T(8,128)(2,1)} async-done(((bf16[384,1024]{1,0:T(8,128)(2,1)}), bf16[384,2048]{1,0:T(8,128)(2,1)}) %all-gather.8.cloned.1.call-update) | async-done | bytes 1572880 | tf_op jit(solution)/shard_map/all_gather | solution.py:88
  227.5 155.4 %all-gather.10.cloned.1.call-done = bf16[2048,3072]{1,0:T(8,128)(2,1)} async-done(((bf16[128,3072]{1,0:T(8,128)(2,1)}), bf16[2048,3072]{1,0:T(8,128)(2,1)}) %all-gather.10.cloned.1.call-update) | async-done | bytes 12582928 | tf_op jit(solution)/shard_map/all_gather | solution.py:91
  382.9 9.9 %fusion.32 = f32[384,3072]{1,0:T(8,128)} fusion(bf16[384,2048]{1,0:T(8,128)(2,1)} %all-gather.8.cloned.1.call-done, bf16[2048,3072]{1,0:T(8,128)(2,1)} %all-gather.10.cloned.1.call-done), kind=kOutput, calls=%fused_computation.73 | convolution fusion | flops 4831838208 | bytes 18874368 | tf_op jit(solution)/shard_map/dot_general | solution.py:89
  392.7 142.4 %all-gather.12.cloned.1.call-done = bf16[2048,3072]{1,0:T(8,128)(2,1)} async-done(((bf16[128,3072]{1,0:T(8,128)(2,1)}), bf16[2048,3072]{1,0:T(8,128)(2,1)}) %all-gather.12.cloned.1.call-update) | async-done | bytes 12582928 | tf_op jit(solution)/shard_map/all_gather | solution.py:96
  535.1 196.2 %all-gather.14.cloned.1.call-done = bf16[3072,2048]{1,0:T(8,128)(2,1)} async-done(((bf16[3072,128]{1,0:T(8,128)(2,1)}), bf16[3072,2048]{1,0:T(8,128)(2,1)}) %all-gather.14.cloned.1.call-update) | async-done | bytes 12582928 | tf_op jit(solution)/shard_map/all_gather | solution.py:102
  731.3 21.0 %convolution_convert_fusion = bf16[384,2048]{1,0:T(8,128)(2,1)} fusion(bf16[3072,2048]{1,0:T(8,128)(2,1)} %all-gather.14.cloned.1.call-done, f32[384,3072]{1,0:T(8,128)} %fusion.32, bf16[384,2048]{1,0:T(8,128)(2,1)S(1)} %copy-done.13, bf16[2048,3072]{1,0:T(8,128)(2,1)} %all-gather.12.cloned.1.call-done), kind=kOutput, calls=%fused_computation.20 | convolution fusion | flops 9671540736 | bytes 33030144 | tf_op jit(solution)/shard_map/dot_general | solution.py:100
  752.3 7.3 reduce-scatter.2.cloned.1.call-done
  (101 shorter events, 72.3 us)
Async XLA Ops:
  6.5 95.7 %copy-start = (bf16[384,512]{1,0:T(8,128)(2,1)S(1)}, bf16[384,512]{1,0:T(8,128)(2,1)}, u32[]{:S(2)}) copy-start(bf16[384,512]{1,0:T(8,128)(2,1)} %param.17) | copy-start | bytes 1179652
  6.5 201.5 %all-gather.6.cloned.1.call-start = ((), (), s32[]{:S(2)}) async-start(), calls=%async_computation.1 | async-start | bytes 2359296 | tf_op jit(solution)/shard_map/all_gather | solution.py:77
  7.8 19.7 %collective-permute-start.12 = (bf16[384,512]{0,1:T(8,128)(2,1)S(1)}, bf16[384,512]{0,1:T(8,128)(2,1)S(1)}, u32[]{:S(2)}, u32[]{:S(2)}) collective-permute-start(bf16[384,512]{0,1:T(8,128)(2,1)S(1)} %copy.26), channel_id=1, source_target_pairs={{0,2},{2,4},{4,6},{6,8},{8,10},{10,12},{12,14},{14,16},{16,18},{18... | collective-permute-start | bytes 1179656 | tf_op jit(solution)/shard_map/ppermute | solution.py:14
  12.7 11.4 %collective-permute-start.4 = (s32[384]{0:T(512)}, s32[384]{0:T(512)S(1)}, u32[]{:S(2)}, u32[]{:S(2)}) collective-permute-start(s32[384]{0:T(512)} %param.21), channel_id=1, source_target_pairs={{0,2},{2,4},{4,6},{6,8},{8,10},{10,12},{12,14},{14,16},{16,18},{18... | collective-permute-start | bytes 4616 | tf_op jit(solution)/shard_map/ppermute | solution.py:14
  16.1 74.4 %collective-permute-start = (bf16[384,1024]{1,0:T(8,128)(2,1)}, bf16[384,1024]{1,0:T(8,128)(2,1)S(1)}, u32[]{:S(2)}, u32[]{:S(2)}) collective-permute-start(bf16[384,1024]{1,0:T(8,128)(2,1)} %param.19), channel_id=1, source_target_pairs={{0,2},{2,4},{4,6},{6,8},{8,10},{10,12},{12,14},{14,16},{16,18},{18... | collective-permute-start | bytes 2359304 | tf_op jit(solution)/shard_map/ppermute | solution.py:14
  20.8 39.8 %collective-permute-start.8 = (bf16[384,512]{0,1:T(8,128)(2,1)S(1)}, bf16[384,512]{0,1:T(8,128)(2,1)S(1)}, u32[]{:S(2)}, u32[]{:S(2)}) collective-permute-start(bf16[384,512]{0,1:T(8,128)(2,1)S(1)} %copy.21), channel_id=1, source_target_pairs={{0,2},{2,4},{4,6},{6,8},{8,10},{10,12},{12,14},{14,16},{16,18},{18... | collective-permute-start | bytes 1179656 | tf_op jit(solution)/shard_map/ppermute | solution.py:14
  24.2 23.4 %collective-permute-start.5 = (s32[384]{0:T(512)S(1)}, s32[384]{0:T(512)S(1)}, u32[]{:S(2)}, u32[]{:S(2)}) collective-permute-start(s32[384]{0:T(512)S(1)} %collective-permute-done.4), channel_id=1, source_target_pairs={{0,2},{2,4},{4,6},{6,8},{8,10},{10,12},{12,14},{14,16},{16,18},{18... | collective-permute-start | bytes 4616 | tf_op jit(solution)/shard_map/ppermute | solution.py:14
  27.6 37.3 %collective-permute-start.13 = (bf16[384,512]{0,1:T(8,128)(2,1)S(1)}, bf16[384,512]{0,1:T(8,128)(2,1)S(1)}, u32[]{:S(2)}, u32[]{:S(2)}) collective-permute-start(bf16[384,512]{0,1:T(8,128)(2,1)S(1)} %collective-permute-done.12), channel_id=1, source_target_pairs={{0,2},{2,4},{4,6},{6,8},{8,10},{10,12},{12,14},{14,16},{16,18},{18... | collective-permute-start | bytes 1179656 | tf_op jit(solution)/shard_map/ppermute | solution.py:14
  47.5 7.3 collective-permute-start.6
  54.9 5.7 collective-permute-start.7
  60.6 13.8 %collective-permute-start.9 = (bf16[384,512]{0,1:T(8,128)(2,1)S(1)}, bf16[384,512]{0,1:T(8,128)(2,1)S(1)}, u32[]{:S(2)}, u32[]{:S(2)}) collective-permute-start(bf16[384,512]{0,1:T(8,128)(2,1)S(1)} %collective-permute-done.8), channel_id=1, source_target_pairs={{0,2},{2,4},{4,6},{6,8},{8,10},{10,12},{12,14},{14,16},{16,18},{18... | collective-permute-start | bytes 1179656 | tf_op jit(solution)/shard_map/ppermute | solution.py:14
  64.9 17.9 %collective-permute-start.14 = (bf16[384,512]{0,1:T(8,128)(2,1)S(1)}, bf16[384,512]{0,1:T(8,128)(2,1)S(1)}, u32[]{:S(2)}, u32[]{:S(2)}) collective-permute-start(bf16[384,512]{0,1:T(8,128)(2,1)S(1)} %collective-permute-done.13), channel_id=1, source_target_pairs={{0,2},{2,4},{4,6},{6,8},{8,10},{10,12},{12,14},{14,16},{16,18},{18... | collective-permute-start | bytes 1179656 | tf_op jit(solution)/shard_map/ppermute | solution.py:14
  74.4 21.5 %collective-permute-start.10 = (bf16[384,512]{0,1:T(8,128)(2,1)S(1)}, bf16[384,512]{0,1:T(8,128)(2,1)}, u32[]{:S(2)}, u32[]{:S(2)}) collective-permute-start(bf16[384,512]{0,1:T(8,128)(2,1)S(1)} %collective-permute-done.9), channel_id=1, source_target_pairs={{0,2},{2,4},{4,6},{6,8},{8,10},{10,12},{12,14},{14,16},{16,18},{18... | collective-permute-start | bytes 1179656 | tf_op jit(solution)/shard_map/ppermute | solution.py:14
  82.8 17.1 %collective-permute-start.15 = (bf16[384,512]{0,1:T(8,128)(2,1)S(1)}, bf16[384,512]{0,1:T(8,128)(2,1)S(1)}, u32[]{:S(2)}, u32[]{:S(2)}) collective-permute-start(bf16[384,512]{0,1:T(8,128)(2,1)S(1)} %collective-permute-done.14), channel_id=1, source_target_pairs={{0,2},{2,4},{4,6},{6,8},{8,10},{10,12},{12,14},{14,16},{16,18},{18... | collective-permute-start | bytes 1179656 | tf_op jit(solution)/shard_map/ppermute | solution.py:14
  90.5 35.3 %collective-permute-start.1 = (bf16[384,1024]{1,0:T(8,128)(2,1)S(1)}, bf16[384,1024]{1,0:T(8,128)(2,1)S(1)}, u32[]{:S(2)}, u32[]{:S(2)}) collective-permute-start(bf16[384,1024]{1,0:T(8,128)(2,1)S(1)} %collective-permute-done), channel_id=1, source_target_pairs={{0,2},{2,4},{4,6},{6,8},{8,10},{10,12},{12,14},{14,16},{16,18},{18... | collective-permute-start | bytes 2359304 | tf_op jit(solution)/shard_map/ppermute | solution.py:14
  95.8 35.5 %collective-permute-start.11 = (bf16[384,512]{0,1:T(8,128)(2,1)}, bf16[384,512]{0,1:T(8,128)(2,1)}, u32[]{:S(2)}, u32[]{:S(2)}) collective-permute-start(bf16[384,512]{0,1:T(8,128)(2,1)} %collective-permute-done.10), channel_id=1, source_target_pairs={{0,2},{2,4},{4,6},{6,8},{8,10},{10,12},{12,14},{14,16},{16,18},{18... | collective-permute-start | bytes 1179656 | tf_op jit(solution)/shard_map/ppermute | solution.py:14
  125.7 17.4 %collective-permute-start.2 = (bf16[384,1024]{1,0:T(8,128)(2,1)S(1)}, bf16[384,1024]{1,0:T(8,128)(2,1)S(1)}, u32[]{:S(2)}, u32[]{:S(2)}) collective-permute-start(bf16[384,1024]{1,0:T(8,128)(2,1)S(1)} %collective-permute-done.1), channel_id=1, source_target_pairs={{0,2},{2,4},{4,6},{6,8},{8,10},{10,12},{12,14},{14,16},{16,18},{18... | collective-permute-start | bytes 2359304 | tf_op jit(solution)/shard_map/ppermute | solution.py:14
  143.1 23.2 %collective-permute-start.3 = (bf16[384,1024]{1,0:T(8,128)(2,1)S(1)}, bf16[384,1024]{1,0:T(8,128)(2,1)S(1)}, u32[]{:S(2)}, u32[]{:S(2)}) collective-permute-start(bf16[384,1024]{1,0:T(8,128)(2,1)S(1)} %collective-permute-done.2), channel_id=1, source_target_pairs={{0,2},{2,4},{4,6},{6,8},{8,10},{10,12},{12,14},{14,16},{16,18},{18... | collective-permute-start | bytes 2359304 | tf_op jit(solution)/shard_map/ppermute | solution.py:14
  193.4 34.1 %all-gather.8.cloned.1.call-start = ((), (), s32[]{:S(2)}) async-start(), calls=%async_computation.2 | async-start | bytes 2359296 | tf_op jit(solution)/shard_map/all_gather | solution.py:88
  216.3 166.5 %all-gather.10.cloned.1.call-start = ((), (), s32[]{:S(2)}) async-start(), calls=%async_computation.3 | async-start | bytes 13369344 | tf_op jit(solution)/shard_map/all_gather | solution.py:91
  217.1 318.1 %all-gather.12.cloned.1.call-start = ((), (), s32[]{:S(2)}) async-start(), calls=%async_computation.4 | async-start | bytes 13369344 | tf_op jit(solution)/shard_map/all_gather | solution.py:96
  217.6 513.7 %all-gather.14.cloned.1.call-start = ((), (), s32[]{:S(2)}) async-start(), calls=%async_computation.5 | async-start | bytes 13369344 | tf_op jit(solution)/shard_map/all_gather | solution.py:102
  218.2 541.4 %reduce-scatter.2.cloned.1.call-start = ((), (), s32[]{:S(2)}) async-start(), calls=%async_computation.6 | async-start | bytes 2359296 | tf_op jit(solution)/shard_map/reduce_scatter | solution.py:105
  227.4 503.9 %copy-start.13 = (bf16[384,2048]{1,0:T(8,128)(2,1)S(1)}, bf16[384,2048]{1,0:T(8,128)(2,1)}, u32[]{:S(2)}) copy-start(bf16[384,2048]{1,0:T(8,128)(2,1)} %all-gather.8.cloned.1.call-done) | copy-start | bytes 4718596
  (14 other events, 293.2 us)
Sparse Core Ops, SparseCore 0:
  193.5 14.5 all-gather.5
  216.4 10.9 all-gather.7
  230.2 152.5 all-gather.9
  385.5 149.5 all-gather.11
  537.7 193.6 all-gather.13
  752.5 7.1 reduce-scatter.1
where the time goes:
time: 770 us; the launch traced here: 769 us
  waiting for transfers between devices  556 us (72%)
  starting transfers between devices  71.9 us (9%)
  matrix products  62.5 us (8%)
  other arithmetic  42.2 us (5%)
  local copies, waits for them, and re-layouts  19.9 us (3%)
  between operations  13.9 us (2%)
    all_gather x1, waiting for transfers between devices, body(): lax.all_gather(down_weight, 'sp', axis=1, tiled=True)  196 us
    all_gather x1, waiting for transfers between devices, body(): lax.all_gather(gate_weight, 'sp', axis=0, tiled=True)  155 us
    all_gather x1, waiting for transfers between devices, body(): lax.all_gather(up_weight, 'sp', axis=0, tiled=True)  142 us
    ppermute x16, starting transfers between devices, shifted(): return lax.ppermute(value, axis, pairs)  71.5 us
    sub x2, other arithmetic, weights(): score = score - jnp.max(score, axis=-1, keepdims=True)  35.1 us
    ppermute x16, waiting for transfers between devices, shifted(): return lax.ppermute(value, axis, pairs)  29.3 us
    dot_general x1, matrix products, body(): jnp.dot(hidden, lax.all_gather(down_weight, 'sp', axis=1, tiled=True), pr...  21 us
  transfers between devices with their start and end apart: 22, of which 12 were waited for; matrix products, arithmetic and copies ran while one was open for 9% of the time, Pallas kernels for 0%

commit v1 on v0

--- a/solution.py
+++ b/solution.py
@@ -1,3 +1,4 @@
+import functools
 import jax
 import jax.numpy as jnp
 from jax import lax
@@ -6,6 +7,13 @@
 HD = 128
 VD = 256
 REACH = 4
+
+
+def handle_shelves_now(payload, which_axis):
+    return jnp.concatenate(lax.all_gather(payload, which_axis), axis=1)
+
+
+view_strips_all = functools.partial(handle_shelves_now, which_axis="sp")
 
 
 def shifted(value, axis, by):
@@ -97,11 +105,7 @@
         preferred_element_type=jnp.float32,
     )
     hidden = (jax.nn.silu(gate) * up).astype(jnp.bfloat16)
-    terms = jnp.dot(
-        hidden,
-        lax.all_gather(down_weight, "sp", axis=1, tiled=True),
-        preferred_element_type=jnp.float32,
-    )
+    terms = jnp.dot(hidden, view_strips_all(down_weight), preferred_element_type=jnp.float32)
     summed = lax.psum_scatter(
         terms.astype(jnp.bfloat16), "tp", scatter_dimension=1, tiled=True
     ).astype(jnp.float32)

time: 770 us -> 715 us (0.929)
  waiting for transfers between devices: 556 us -> 489 us
  local copies, waits for them, and re-layouts: 19.9 us -> 36.6 us
    all_gather x1, waiting for transfers between devices: 196 us -> 146 us  [handle_shelves_now(): return jnp.concatenate(lax.all_gather(payload, which_axis), axis=1)]
    reshape x0 -> x1, local copies, waits for them, and re-layouts: none -> 16.7 us  [handle_shelves_now(): return jnp.concatenate(lax.all_gather(payload, which_axis), axis=1)]
    all_gather x1, waiting for transfers between devices: 9.18 us -> 0.01 us  [body(): whole_rows = lax.all_gather(normed, 'tp', axis=1, tiled=True)]
  transfers between devices with their start and end apart: 22 -> 22, of which waited for: 12 -> 11; matrix products, arithmetic and copies ran while one was open for 9% -> 13% of each run, Pallas kernels for 0% -> 0%
where the time goes in v1:
time: 715 us; the launch traced here: 713 us
  waiting for transfers between devices  489 us (68%)
  starting transfers between devices  71.9 us (10%)
  matrix products  57.7 us (8%)
  other arithmetic  42.2 us (6%)
  local copies, waits for them, and re-layouts  36.6 us (5%)
  between operations  13.9 us (2%)
    all_gather x1, waiting for transfers between devices, body(): lax.all_gather(gate_weight, 'sp', axis=0, tiled=True)  148 us
    all_gather x1, waiting for transfers between devices, handle_shelves_now(): return jnp.concatenate(lax.all_gather(payload, which_axis), axis=1)  146 us
    all_gather x1, waiting for transfers between devices, body(): lax.all_gather(up_weight, 'sp', axis=0, tiled=True)  142 us
    ppermute x16, starting transfers between devices, shifted(): return lax.ppermute(value, axis, pairs)  71.5 us
    sub x2, other arithmetic, weights(): score = score - jnp.max(score, axis=-1, keepdims=True)  35 us
    ppermute x16, waiting for transfers between devices, shifted(): return lax.ppermute(value, axis, pairs)  29.3 us
    reshape x1, local copies, waits for them, and re-layouts, handle_shelves_now(): return jnp.concatenate(lax.all_gather(payload, which_axis), axis=1)  16.7 us
    dot_general x1, matrix products, body(): jnp.dot(hidden, view_strips_all(down_weight), preferred_element_type=jnp....  16.3 us
  transfers between devices with their start and end apart: 22, of which 11 were waited for; matrix products, arithmetic and copies ran while one was open for 13% of the time, Pallas kernels for 0%

profile of v1, /device:TPU:0, one launch (start us, length us, event | category | flops | bytes accessed | tf_op | source)
XLA Modules:
  0.0 713.3 jit_solution(3571459627119220905)
XLA Ops:
  7.8 4.9 collective-permute-start.12
  31.0 16.5 %collective-permute-done.5 = s32[384]{0:T(512)S(1)} collective-permute-done((s32[384]{0:T(512)S(1)}, s32[384]{0:T(512)S(1)}, u32[]{:S(2)}, u32[]{:S(2)}) %collective-permute-start.5) | collective-permute-done | bytes 1568 | tf_op jit(solution)/shard_map/ppermute | solution.py:22
  64.9 5.1 collective-permute-start.14
  74.4 5.9 collective-permute-start.10
  82.8 5.1 collective-permute-start.15
  90.5 5.3 collective-permute-start.1
  102.2 6.2 fusion.19
  108.4 17.4 %fusion.30 = (f32[4,384]{1,0:T(4,128)S(1)}, f32[4,384,1920]{1,2,0:T(8,128)}) fusion(f32[4,1920,384]{2,1,0:T(8,128)} %fusion.19, pred[384,1920]{0,1:T(8,128)(4,1)S(1)} %and_and_fusion), kind=kOutput, calls=%fused_computation.71 | output fusion | flops 17696640 | bytes 24336384 | tf_op jit(solution)/shard_map/sub | solution.py:67
  125.7 5.6 collective-permute-start.2
  134.7 6.1 fusion.22
  143.1 5.5 collective-permute-start.3
  148.6 17.7 %fusion.31 = (f32[4,384]{1,0:T(4,128)S(1)}, f32[4,384,1920]{1,2,0:T(8,128)}) fusion(f32[4,1920,384]{2,1,0:T(8,128)} %fusion.22, pred[384,1920]{0,1:T(8,128)(4,1)} %copy-done.4), kind=kOutput, calls=%fused_computation.72 | output fusion | flops 17696640 | bytes 24336384 | tf_op jit(solution)/shard_map/sub | solution.py:67
  171.1 6.3 copy.31
  177.4 8.0 %fusion.9 = f32[4,256,384]{2,1,0:T(8,128)S(1)} fusion(bf16[1920,4,256]{0,2,1:T(8,128)(2,1)} %bitcast.66, f32[4,384,1920]{1,2,0:T(8,128)} %get-tuple-element.6, f32[4,384]{1,0:T(4,128)S(1)} %get-tuple-element.5), kind=kOutput, calls=%fused_computation.15 | convolution fusion | flops 1515847680 | bytes 17307648 | tf_op jit(solution)/shard_map/hqk,khe->qhe/dot_general | solution.py:74
  185.4 6.7 fusion.16
  194.3 13.7 %all-gather.7.cloned.1.call-done = bf16[384,2048]{0,1:T(8,128)(2,1)} async-done(((bf16[384,1024]{0,1:T(8,128)(2,1)}), bf16[384,2048]{0,1:T(8,128)(2,1)}) %all-gather.7.cloned.1.call-update) | async-done | bytes 1572880 | tf_op jit(solution)/shard_map/all_gather | solution.py:85
  208.0 4.6 fusion.12
  217.4 145.9 %all-gather.15.cloned.1.call-done = bf16[49152,128]{1,0:T(8,128)(2,1)} async-done(((bf16[3072,128]{1,0:T(8,128)(2,1)}), bf16[49152,128]{1,0:T(8,128)(2,1)}) %all-gather.15.cloned.1.call-update) | async-done | bytes 12582928 | tf_op jit(solution)/shard_map/all_gather | solution.py:13
  363.4 16.7 %copy.42 = bf16[3072,16,128]{0,2,1:T(8,128)(2,1)} copy(bf16[3072,16,128]{2,0,1:T(8,128)(2,1)} %bitcast.64) | data formatting | bytes 25165824 | tf_op jit(solution)/shard_map/reshape | solution.py:13
  380.1 148.1 %all-gather.11.cloned.1.call-done = bf16[2048,3072]{1,0:T(8,128)(2,1)} async-done(((bf16[128,3072]{1,0:T(8,128)(2,1)}), bf16[2048,3072]{1,0:T(8,128)(2,1)}) %all-gather.11.cloned.1.call-update) | async-done | bytes 12582928 | tf_op jit(solution)/shard_map/all_gather | solution.py:99
  528.2 9.9 %fusion.32 = f32[384,3072]{1,0:T(8,128)} fusion(bf16[384,2048]{1,0:T(8,128)(2,1)} %all-gather.9.cloned.1.call-done, bf16[2048,3072]{1,0:T(8,128)(2,1)} %all-gather.11.cloned.1.call-done), kind=kOutput, calls=%fused_computation.73 | convolution fusion | flops 4831838208 | bytes 18874368 | tf_op jit(solution)/shard_map/dot_general | solution.py:97
  538.0 142.4 %all-gather.13.cloned.1.call-done = bf16[2048,3072]{1,0:T(8,128)(2,1)} async-done(((bf16[128,3072]{1,0:T(8,128)(2,1)}), bf16[2048,3072]{1,0:T(8,128)(2,1)}) %all-gather.13.cloned.1.call-update) | async-done | bytes 12582928 | tf_op jit(solution)/shard_map/all_gather | solution.py:104
  680.4 16.3 %convolution_convert_fusion = bf16[384,2048]{1,0:T(8,128)(2,1)} fusion(bf16[3072,2048]{0,1:T(8,128)(2,1)} %bitcast.65, f32[384,3072]{1,0:T(8,128)} %fusion.32, bf16[384,2048]{1,0:T(8,128)(2,1)S(1)} %copy-done.13, bf16[2048,3072]{1,0:T(8,128)(2,1)} %all-gather.13.cloned.1.call-done), kind=kOutput, calls=%fused_computation.20 | convolution fusion | flops 9671540736 | bytes 33030144 | tf_op jit(solution)/shard_map/dot_general | solution.py:108
  696.8 7.3 %reduce-scatter.2.cloned.1.call-done = bf16[384,1024]{1,0:T(8,128)(2,1)} async-done(((bf16[384,2048]{1,0:T(8,128)(2,1)}), bf16[384,1024]{1,0:T(8,128)(2,1)}) %reduce-scatter.2.cloned.1.call-update) | async-done | bytes 786448 | tf_op jit(solution)/shard_map/reduce_scatter | solution.py:109
  (102 shorter events, 72.3 us)
Async XLA Ops:
  6.5 95.7 %copy-start = (bf16[384,512]{1,0:T(8,128)(2,1)S(1)}, bf16[384,512]{1,0:T(8,128)(2,1)}, u32[]{:S(2)}) copy-start(bf16[384,512]{1,0:T(8,128)(2,1)} %param.17) | copy-start | bytes 1179652
  6.5 201.4 %all-gather.7.cloned.1.call-start = ((), (), s32[]{:S(2)}) async-start(), calls=%async_computation.1 | async-start | bytes 2359296 | tf_op jit(solution)/shard_map/all_gather | solution.py:85
  7.8 19.7 %collective-permute-start.12 = (bf16[384,512]{0,1:T(8,128)(2,1)S(1)}, bf16[384,512]{0,1:T(8,128)(2,1)S(1)}, u32[]{:S(2)}, u32[]{:S(2)}) collective-permute-start(bf16[384,512]{0,1:T(8,128)(2,1)S(1)} %copy.37), channel_id=1, source_target_pairs={{0,2},{2,4},{4,6},{6,8},{8,10},{10,12},{12,14},{14,16},{16,18},{18... | collective-permute-start | bytes 1179656 | tf_op jit(solution)/shard_map/ppermute | solution.py:22
  12.7 11.4 %collective-permute-start.4 = (s32[384]{0:T(512)}, s32[384]{0:T(512)S(1)}, u32[]{:S(2)}, u32[]{:S(2)}) collective-permute-start(s32[384]{0:T(512)} %param.21), channel_id=1, source_target_pairs={{0,2},{2,4},{4,6},{6,8},{8,10},{10,12},{12,14},{14,16},{16,18},{18... | collective-permute-start | bytes 4616 | tf_op jit(solution)/shard_map/ppermute | solution.py:22
  16.1 74.4 %collective-permute-start = (bf16[384,1024]{1,0:T(8,128)(2,1)}, bf16[384,1024]{1,0:T(8,128)(2,1)S(1)}, u32[]{:S(2)}, u32[]{:S(2)}) collective-permute-start(bf16[384,1024]{1,0:T(8,128)(2,1)} %param.19), channel_id=1, source_target_pairs={{0,2},{2,4},{4,6},{6,8},{8,10},{10,12},{12,14},{14,16},{16,18},{18... | collective-permute-start | bytes 2359304 | tf_op jit(solution)/shard_map/ppermute | solution.py:22
  20.8 39.8 %collective-permute-start.8 = (bf16[384,512]{0,1:T(8,128)(2,1)S(1)}, bf16[384,512]{0,1:T(8,128)(2,1)S(1)}, u32[]{:S(2)}, u32[]{:S(2)}) collective-permute-start(bf16[384,512]{0,1:T(8,128)(2,1)S(1)} %copy.32), channel_id=1, source_target_pairs={{0,2},{2,4},{4,6},{6,8},{8,10},{10,12},{12,14},{14,16},{16,18},{18... | collective-permute-start | bytes 1179656 | tf_op jit(solution)/shard_map/ppermute | solution.py:22
  24.2 23.4 %collective-permute-start.5 = (s32[384]{0:T(512)S(1)}, s32[384]{0:T(512)S(1)}, u32[]{:S(2)}, u32[]{:S(2)}) collective-permute-start(s32[384]{0:T(512)S(1)} %collective-permute-done.4), channel_id=1, source_target_pairs={{0,2},{2,4},{4,6},{6,8},{8,10},{10,12},{12,14},{14,16},{16,18},{18... | collective-permute-start | bytes 4616 | tf_op jit(solution)/shard_map/ppermute | solution.py:22
  27.6 37.3 %collective-permute-start.13 = (bf16[384,512]{0,1:T(8,128)(2,1)S(1)}, bf16[384,512]{0,1:T(8,128)(2,1)S(1)}, u32[]{:S(2)}, u32[]{:S(2)}) collective-permute-start(bf16[384,512]{0,1:T(8,128)(2,1)S(1)} %collective-permute-done.12), channel_id=1, source_target_pairs={{0,2},{2,4},{4,6},{6,8},{8,10},{10,12},{12,14},{14,16},{16,18},{18... | collective-permute-start | bytes 1179656 | tf_op jit(solution)/shard_map/ppermute | solution.py:22
  47.5 7.3 %collective-permute-start.6 = (s32[384]{0:T(512)S(1)}, s32[384]{0:T(512)S(1)}, u32[]{:S(2)}, u32[]{:S(2)}) collective-permute-start(s32[384]{0:T(512)S(1)} %collective-permute-done.5), channel_id=1, source_target_pairs={{0,2},{2,4},{4,6},{6,8},{8,10},{10,12},{12,14},{14,16},{16,18},{18... | collective-permute-start | bytes 4616 | tf_op jit(solution)/shard_map/ppermute | solution.py:22
  54.9 5.7 collective-permute-start.7
  60.6 13.8 %collective-permute-start.9 = (bf16[384,512]{0,1:T(8,128)(2,1)S(1)}, bf16[384,512]{0,1:T(8,128)(2,1)S(1)}, u32[]{:S(2)}, u32[]{:S(2)}) collective-permute-start(bf16[384,512]{0,1:T(8,128)(2,1)S(1)} %collective-permute-done.8), channel_id=1, source_target_pairs={{0,2},{2,4},{4,6},{6,8},{8,10},{10,12},{12,14},{14,16},{16,18},{18... | collective-permute-start | bytes 1179656 | tf_op jit(solution)/shard_map/ppermute | solution.py:22
  64.9 17.9 %collective-permute-start.14 = (bf16[384,512]{0,1:T(8,128)(2,1)S(1)}, bf16[384,512]{0,1:T(8,128)(2,1)S(1)}, u32[]{:S(2)}, u32[]{:S(2)}) collective-permute-start(bf16[384,512]{0,1:T(8,128)(2,1)S(1)} %collective-permute-done.13), channel_id=1, source_target_pairs={{0,2},{2,4},{4,6},{6,8},{8,10},{10,12},{12,14},{14,16},{16,18},{18... | collective-permute-start | bytes 1179656 | tf_op jit(solution)/shard_map/ppermute | solution.py:22
  74.4 21.5 %collective-permute-start.10 = (bf16[384,512]{0,1:T(8,128)(2,1)S(1)}, bf16[384,512]{0,1:T(8,128)(2,1)}, u32[]{:S(2)}, u32[]{:S(2)}) collective-permute-start(bf16[384,512]{0,1:T(8,128)(2,1)S(1)} %collective-permute-done.9), channel_id=1, source_target_pairs={{0,2},{2,4},{4,6},{6,8},{8,10},{10,12},{12,14},{14,16},{16,18},{18... | collective-permute-start | bytes 1179656 | tf_op jit(solution)/shard_map/ppermute | solution.py:22
  82.8 17.1 %collective-permute-start.15 = (bf16[384,512]{0,1:T(8,128)(2,1)S(1)}, bf16[384,512]{0,1:T(8,128)(2,1)S(1)}, u32[]{:S(2)}, u32[]{:S(2)}) collective-permute-start(bf16[384,512]{0,1:T(8,128)(2,1)S(1)} %collective-permute-done.14), channel_id=1, source_target_pairs={{0,2},{2,4},{4,6},{6,8},{8,10},{10,12},{12,14},{14,16},{16,18},{18... | collective-permute-start | bytes 1179656 | tf_op jit(solution)/shard_map/ppermute | solution.py:22
  90.5 35.3 %collective-permute-start.1 = (bf16[384,1024]{1,0:T(8,128)(2,1)S(1)}, bf16[384,1024]{1,0:T(8,128)(2,1)S(1)}, u32[]{:S(2)}, u32[]{:S(2)}) collective-permute-start(bf16[384,1024]{1,0:T(8,128)(2,1)S(1)} %collective-permute-done), channel_id=1, source_target_pairs={{0,2},{2,4},{4,6},{6,8},{8,10},{10,12},{12,14},{14,16},{16,18},{18... | collective-permute-start | bytes 2359304 | tf_op jit(solution)/shard_map/ppermute | solution.py:22
  95.8 35.5 %collective-permute-start.11 = (bf16[384,512]{0,1:T(8,128)(2,1)}, bf16[384,512]{0,1:T(8,128)(2,1)}, u32[]{:S(2)}, u32[]{:S(2)}) collective-permute-start(bf16[384,512]{0,1:T(8,128)(2,1)} %collective-permute-done.10), channel_id=1, source_target_pairs={{0,2},{2,4},{4,6},{6,8},{8,10},{10,12},{12,14},{14,16},{16,18},{18... | collective-permute-start | bytes 1179656 | tf_op jit(solution)/shard_map/ppermute | solution.py:22
  125.7 17.4 %collective-permute-start.2 = (bf16[384,1024]{1,0:T(8,128)(2,1)S(1)}, bf16[384,1024]{1,0:T(8,128)(2,1)S(1)}, u32[]{:S(2)}, u32[]{:S(2)}) collective-permute-start(bf16[384,1024]{1,0:T(8,128)(2,1)S(1)} %collective-permute-done.1), channel_id=1, source_target_pairs={{0,2},{2,4},{4,6},{6,8},{8,10},{10,12},{12,14},{14,16},{16,18},{18... | collective-permute-start | bytes 2359304 | tf_op jit(solution)/shard_map/ppermute | solution.py:22
  143.1 23.2 %collective-permute-start.3 = (bf16[384,1024]{1,0:T(8,128)(2,1)S(1)}, bf16[384,1024]{1,0:T(8,128)(2,1)S(1)}, u32[]{:S(2)}, u32[]{:S(2)}) collective-permute-start(bf16[384,1024]{1,0:T(8,128)(2,1)S(1)} %collective-permute-done.2), channel_id=1, source_target_pairs={{0,2},{2,4},{4,6},{6,8},{8,10},{10,12},{12,14},{14,16},{16,18},{18... | collective-permute-start | bytes 2359304 | tf_op jit(solution)/shard_map/ppermute | solution.py:22
  193.2 170.1 %all-gather.15.cloned.1.call-start = ((), (), s32[]{:S(2)}) async-start(), calls=%async_computation.6 | async-start | bytes 13369344 | tf_op jit(solution)/shard_map/all_gather | solution.py:13
  194.0 186.1 %all-gather.9.cloned.1.call-start = ((), (), s32[]{:S(2)}) async-start(), calls=%async_computation.2 | async-start | bytes 2359296 | tf_op jit(solution)/shard_map/all_gather | solution.py:96
  216.2 312.0 %all-gather.11.cloned.1.call-start = ((), (), s32[]{:S(2)}) async-start(), calls=%async_computation.3 | async-start | bytes 13369344 | tf_op jit(solution)/shard_map/all_gather | solution.py:99
  216.8 463.6 %all-gather.13.cloned.1.call-start = ((), (), s32[]{:S(2)}) async-start(), calls=%async_computation.4 | async-start | bytes 13369344 | tf_op jit(solution)/shard_map/all_gather | solution.py:104
  217.4 486.7 %reduce-scatter.2.cloned.1.call-start = ((), (), s32[]{:S(2)}) async-start(), calls=%async_computation.5 | async-start | bytes 2359296 | tf_op jit(solution)/shard_map/reduce_scatter | solution.py:109
  380.1 300.4 %copy-start.13 = (bf16[384,2048]{1,0:T(8,128)(2,1)S(1)}, bf16[384,2048]{1,0:T(8,128)(2,1)}, u32[]{:S(2)}) copy-start(bf16[384,2048]{1,0:T(8,128)(2,1)} %all-gather.9.cloned.1.call-done) | copy-start | bytes 4718596
  (14 other events, 280.9 us)
Sparse Core Ops, SparseCore 0:
  193.4 14.5 all-gather.6
  210.7 152.5 all-gather.14
  364.9 7.9 all-gather.8
  375.6 152.5 all-gather.10
  530.8 149.5 all-gather.12
  696.9 7.1 reduce-scatter.1
